TPU v7x, 32 devices: a whole 2x2x4 slice. The times are simulated.
32 devices in a mesh: grp: 2 (over y), ep: 8 (over z, x), tp: 2 (over core).
Axes of the slice: x: 2, y: 2, z: 4, core: 2. Of those that a mesh axis runs over, the one named last changes fastest.
Arguments:
- tokens: bfloat16 [512, 2048], P(('grp', 'ep'), 'tp'), parts along dimension 0, may hold values from -6 to 6
- gain: float32 [2048], replicated, may hold values from 0.1 to 1.9
- routes: int32 [512, 4], P(('grp', 'ep')), parts along dimension 0, may hold values from 0 to 7, all different within a row; in each aligned block of 32 rows (0 to 31, 32 to 63, ...) at most 32 rows name the same one
- weights: float32 [512, 4], P(('grp', 'ep')), parts along dimension 0, may hold values from 0.05 to 1
- w_gate: bfloat16 [8, 2048, 6144], P('ep', None, 'tp'), may hold values from -0.125 to 0.125
- w_up: bfloat16 [8, 2048, 6144], P('ep', None, 'tp'), may hold values from -0.125 to 0.125
- w_down: bfloat16 [8, 6144, 2048], P('ep', 'tp'), may hold values from -0.078125 to 0.078125
Outputs:
- mixed: bfloat16 [512, 2048], P(('grp', 'ep'), 'tp'), parts along dimension 0
There are 2 independent parts, one for each index of `grp`. A program takes and returns all parts, laid end to end along the dimension named above; an argument that names none is the same for every part. Nothing has to cross between parts.
Inputs may be any that keep to these rules, and one draw needn't show every extreme that they name: `routes`: each row names 4 different experts. Among the rows of one device no expert is named by more than 32 rows, a bound that some block reaches.
All inputs are finite; a program needn't handle non-finite values.
Results may differ from a plain program's by a relative error of at most 0.019.
Values may be sent and summed in bfloat16 or wider, within the bound.
A program may use at most 128 MiB of HBM per device.

v0:
```python
import jax
import jax.numpy as jnp
from jax import lax
from jax.sharding import PartitionSpec as P

epsilon = 1e-05


def expert_rows(chosen, gate_w, up_w, down_w):
    gate_val = jnp.dot(chosen, gate_w, preferred_element_type=jnp.float32)
    up_val = jnp.dot(chosen, up_w, preferred_element_type=jnp.float32)
    hidden = (jax.nn.silu(gate_val) * up_val).astype(jnp.bfloat16)
    partial_value = jnp.dot(hidden, down_w, preferred_element_type=jnp.float32).astype(jnp.bfloat16)
    return (
        lax.psum_scatter(partial_value, "tp", scatter_dimension=1, tiled=True)
        .astype(jnp.float32)
        .astype(jnp.bfloat16)
    )


def on_device(tokens, gain, routes, weights, w_gate, w_up, w_down):
    groups = lax.axis_size("ep")
    shards = lax.axis_size("tp")
    tok_rows, top_count = routes.shape
    capacity = min(tok_rows, 2 * tok_rows * top_count // groups)
    gate_w, up_w, down_w = (w_gate[0], w_up[0], w_down[0])
    values = tokens.astype(jnp.float32)
    own_width = values.shape[1]
    width = own_width * shards
    totals = lax.psum((jnp.sum(values, axis=1), jnp.sum(values * values, axis=1)), "tp")
    average = totals[0] / width
    spread = totals[1] / width - average * average
    local_gain = lax.dynamic_slice_in_dim(gain, lax.axis_index("tp") * own_width, own_width)
    normed = (
        (values - average[:, None]) * lax.rsqrt(spread[:, None] + epsilon) * local_gain
    ).astype(jnp.bfloat16)
    pair_expert = routes.reshape(-1)
    pair_token = jnp.arange(tok_rows * top_count, dtype=jnp.int32) // top_count
    member = (pair_expert[:, None] == jnp.arange(groups, dtype=jnp.int32)[None, :]).astype(
        jnp.int32
    )
    earlier = jnp.cumsum(member, axis=0) - member
    position = pair_expert * capacity + jnp.sum(earlier * member, axis=1)
    row_width = normed.shape[1]
    outbox = (
        jnp.zeros((groups * capacity, row_width), jnp.bfloat16).at[position].set(normed[pair_token])
    )
    outbox = outbox.reshape(groups, capacity, row_width)
    arrived = lax.all_gather(
        lax.all_to_all(outbox, "ep", split_axis=0, concat_axis=0, tiled=True),
        "tp",
        axis=2,
        tiled=True,
    )
    count = arrived.shape[1]
    flat_rows = arrived.reshape(groups * count, arrived.shape[2])
    served = expert_rows(flat_rows, gate_w, up_w, down_w).reshape(groups, count, -1)
    returned = lax.all_to_all(served, "ep", split_axis=0, concat_axis=0, tiled=True)
    picked = (
        returned.reshape(groups * capacity, -1)[position]
        .reshape(tok_rows, top_count, -1)
        .astype(jnp.float32)
    )
    return jnp.sum(picked * weights[:, :, None], axis=1).astype(jnp.bfloat16)


def solution(mesh):
    in_specs = (
        P(("grp", "ep"), "tp"),
        P(),
        P(("grp", "ep"), None),
        P(("grp", "ep"), None),
        P("ep", None, "tp"),
        P("ep", None, "tp"),
        P("ep", "tp", None),
    )
    out_specs = P(("grp", "ep"), "tp")
    return jax.shard_map(
        on_device, mesh=mesh, in_specs=in_specs, out_specs=out_specs, check_vma=False
    )
```

profile of v0, /device:TPU:0, one launch (start us, length us, event | category | flops | bytes accessed | tf_op | source)
XLA Modules:
  0.0 112.8 jit_solution(12843658255355050022)
XLA Ops:
  6.5 0.0 all-gather.2.cloned.1.call-start
  6.5 0.8 copy.12
  7.3 0.7 broadcast_multiply_fusion
  8.0 1.0 convert_reduce_fusion
  9.0 0.1 eq.15
  9.1 0.1 fusion.24
  9.2 0.2 reduce_window_sum.11
  9.3 0.2 select_reduce_fusion
  9.5 0.1 copy.11
  9.6 0.1 mul.57
  9.7 2.6 %all-reduce = (f32[32]{0:T(128)S(1)}, f32[32]{0:T(128)S(1)}) all-reduce(f32[32]{0:T(128)S(1)} %get-tuple-element.6, f32[32]{0:T(128)S(1)} %get-tuple-element.5), channel_id=1, replica_groups=mesh['grp'=2,'ep'=8,'tp'=2] {'tp'}, use_global_device_ids=true, to_apply=%region_5.6 | all-reduce | flops 64 | bytes 512 | tf_op jit(solution)/shard_map/psum | solution.py:30
  12.4 0.7 dynamic_slice.3
  13.1 0.9 fusion.22
  14.0 2.2 %scatter_custom_fusion = bf16[256,1024]{1,0:T(8,128)(2,1)S(1)} fusion(s32[128]{0:T(128)S(1)} %fusion.26, bf16[32,1024]{1,0:T(8,128)(2,1)S(1)} %fusion.22, s32[1024]{0:T(1024)S(1)} %pad_clamp_fusion.1, bf16[]{:T(256)} %constant.34.clone.1), kind=kCustom, calls=%fused_computation.13 | custom fusion | bytes 524290 | tf_op jit(solution)/shard_map/scatter | solution.py:46
  16.2 21.8 %all_to_all.10 = bf16[8,32,1024]{2,1,0:T(8,128)(2,1)} all-to-all(bf16[8,32,1024]{2,1,0:T(8,128)(2,1)S(1)} %bitcast.32), channel_id=1, replica_groups=mesh['grp'=2,'ep'=8,'tp'=2] {'ep'}, dimensions={0} | all-to-all | bytes 1048576 | tf_op jit(solution)/shard_map/all_to_all | solution.py:50
  38.0 0.0 all-gather.2.cloned.1.call-update
  38.1 0.0 reduce-scatter.2.cloned.1.call-start
  38.1 8.2 %all-gather.2.cloned.1.call-done = bf16[8,32,2048]{2,1,0:T(8,128)(2,1)} async-done(((bf16[8,32,1024]{2,1,0:T(8,128)(2,1)}), bf16[8,32,2048]{2,1,0:T(8,128)(2,1)}) %all-gather.2.cloned.1.call-update) | async-done | bytes 1048592 | tf_op jit(solution)/shard_map/all_gather | solution.py:49
  46.3 0.0 copy-start.1
  46.3 10.1 %fusion.4 = f32[256,3072]{1,0:T(8,128)} fusion(bf16[256,2048]{1,0:T(8,128)(2,1)} %bitcast.34, bf16[1,2048,3072]{2,1,0:T(8,128)(2,1)} %param.11), kind=kOutput, calls=%fused_computation.7 | convolution fusion | flops 3221225472 | bytes 16777216 | tf_op jit(solution)/shard_map/dot_general | solution.py:10
  56.4 0.0 copy-done.1
  56.4 0.0 copy-start
  56.4 17.0 %fusion.12 = bf16[256,2048]{1,0:T(8,128)(2,1)} fusion(bf16[1,3072,2048]{2,1,0:T(8,128)(2,1)} %param.13, bf16[256,2048]{1,0:T(8,128)(2,1)S(1)} %bitcast.35, bf16[1,2048,3072]{2,1,0:T(8,128)(2,1)} %param.12, f32[256,3072]{1,0:T(8,128)} %fusion.4), kind=kOutput, calls=%fused_computation.11 | convolution fusion | flops 6447693824 | bytes 30408704 | tf_op jit(solution)/shard_map/dot_general | solution.py:13
  73.4 0.0 reduce-scatter.2.cloned.1.call-update
  73.5 9.7 %reduce-scatter.2.cloned.1.call-done = bf16[256,1024]{1,0:T(8,128)(2,1)} async-done(((bf16[256,2048]{1,0:T(8,128)(2,1)}), bf16[256,1024]{1,0:T(8,128)(2,1)}) %reduce-scatter.2.cloned.1.call-update) | async-done | bytes 524304 | tf_op jit(solution)/shard_map/reduce_scatter | solution.py:15
  83.2 5.8 %all-to-all-start.1 = ((bf16[8,32,1024]{2,1,0:T(8,128)(2,1)}), bf16[8,32,1024]{2,1,0:T(8,128)(2,1)S(1)}, u32[]{:S(2)}, u32[]{:S(2)}) async-start(bf16[8,32,1024]{2,1,0:T(8,128)(2,1)} %bitcast.33), calls=%async_computation.2 | async-start | bytes 1048576 | tf_op jit(solution)/shard_map/all_to_all | solution.py:58
  88.9 0.0 copy-done
  88.9 0.1 copy.13
  89.0 14.8 %all-to-all-done.1 = bf16[8,32,1024]{2,1,0:T(8,128)(2,1)S(1)} async-done(((bf16[8,32,1024]{2,1,0:T(8,128)(2,1)}), bf16[8,32,1024]{2,1,0:T(8,128)(2,1)S(1)}, u32[]{:S(2)}, u32[]{:S(2)}) %all-to-all-start.1) | async-done | bytes 524320 | tf_op jit(solution)/shard_map/all_to_all | solution.py:58
  103.9 0.9 gather_fusion
  104.7 0.2 reshape.98
  104.9 1.0 multiply_reduce_fusion
  (5 shorter events, 0.0 us)
Async XLA Ops:
  6.5 39.8 %all-gather.2.cloned.1.call-start = ((), (), s32[]{:S(2)}) async-start(), calls=%async_computation.3 | async-start | bytes 1572864 | tf_op jit(solution)/shard_map/all_gather | solution.py:49
  38.1 45.1 %reduce-scatter.2.cloned.1.call-start = ((), (), s32[]{:S(2)}) async-start(), calls=%async_computation.4 | async-start | bytes 1572864 | tf_op jit(solution)/shard_map/reduce_scatter | solution.py:15
  46.3 10.1 %copy-start.1 = (bf16[8,32,2048]{2,1,0:T(8,128)(2,1)S(1)}, bf16[8,32,2048]{2,1,0:T(8,128)(2,1)}, u32[]{:S(2)}) copy-start(bf16[8,32,2048]{2,1,0:T(8,128)(2,1)} %all-gather.2.cloned.1.call-done) | copy-start | bytes 3145732
  56.4 32.5 %copy-start = (f32[32,4]{0,1:T(4,128)S(1)}, f32[32,4]{0,1:T(4,128)}, u32[]{:S(2)}) copy-start(f32[32,4]{0,1:T(4,128)} %param.10) | copy-start | bytes 1540
  83.2 20.7 %all-to-all-start.1 = ((bf16[8,32,1024]{2,1,0:T(8,128)(2,1)}), bf16[8,32,1024]{2,1,0:T(8,128)(2,1)S(1)}, u32[]{:S(2)}, u32[]{:S(2)}) async-start(bf16[8,32,1024]{2,1,0:T(8,128)(2,1)} %bitcast.33), calls=%async_computation.2 | async-start | bytes 1048576 | tf_op jit(solution)/shard_map/all_to_all | solution.py:58
Sparse Core Ops, SparseCore 0:
  38.2 8.0 all-gather.1
  73.6 9.5 reduce-scatter.1
where the time goes:
time: 113 us
  waiting for transfers between devices  32.8 us (29%)
  matrix products  27.1 us (24%)
  blocking collectives  24.5 us (22%)
  between operations  13.5 us (12%)
  starting transfers between devices  5.82 us (5%)
  local copies, waits for them, and re-layouts  5.08 us (4%)
  other arithmetic  4.06 us (4%)
    all_to_all x1, blocking collectives, on_device(): lax.all_to_all(outbox, 'ep', split_axis=0, concat_axis=0, tiled=True)  21.8 us
    dot_general x1, matrix products, expert_rows(): jnp.dot(hidden, down_w, preferred_element_type=jnp.float32)  17 us
    all_to_all x1, waiting for transfers between devices, on_device(): lax.all_to_all(served, 'ep', split_axis=0, concat_axis=0, tiled=True)  14.8 us
    dot_general x1, matrix products, expert_rows(): gate_val = jnp.dot(chosen, gate_w, preferred_element_type=jnp.float32)  10.1 us
    reduce_scatter x1, waiting for transfers between devices, expert_rows(): lax.psum_scatter(partial_value, 'tp', scatter_dimension=1, tiled=True)  9.7 us
    all_gather x1, waiting for transfers between devices, on_device(): lax.all_gather(lax.all_to_all(outbox, 'ep', split_axis=0, concat_axis=0,...  8.21 us
    all_to_all x1, starting transfers between devices, on_device(): lax.all_to_all(served, 'ep', split_axis=0, concat_axis=0, tiled=True)  5.78 us
    psum x1, blocking collectives, on_device(): lax.psum((jnp.sum(values, axis=1), jnp.sum(values * values, axis=1)), 'tp')  2.63 us
  transfers between devices with their start and end apart: 3, of which 3 were waited for; matrix products, arithmetic and copies ran while one was open for 0% of the time, Pallas kernels for 0%

commit v1 on v0

v1 whole, which is shorter than its diff:
```python
import functools

import jax
import jax.numpy as jnp
from jax import lax
from jax.experimental import pallas as pl
from jax.experimental.pallas import tpu as pltpu
from jax.sharding import PartitionSpec as P

epsilon = 1e-05
MESH = pl.DeviceIdType.MESH
BF = jnp.bfloat16
F32 = jnp.float32


def piece(total, most):
    best = 128
    for cand in range(128, min(total, most) + 1, 128):
        if total % cand == 0:
            best = cand
    return best


def kernel(dims, tok, gain, routes, weights, wg_hbm, wu_hbm, wd_hbm, out,
           xg, normed, hidden, wcol, wsrc, wrow, wg, wu, wd,
           psend, precv, sacc, xsend, xrecv, zsend, zrecv,
           wg_sem, wu_sem, wd_sem, gs, gr, ws, wr, ps, pr, xs, xr, zs, zr):
    n_ep, n_tp, X, Z, rows, w, FC, NF, CW, J, top = dims
    e = lax.axis_index("ep")
    t = lax.axis_index("tp")
    x = lax.rem(e, X)
    z = e // X
    xp = X - 1 - x

    def w_copy(kind, c):
        if kind == 2:
            return pltpu.make_async_copy(wd_hbm.at[0, :, pl.ds(c * CW, CW)], wd.at[c], wd_sem.at[c])
        src, dst, sem = ((wg_hbm, wg, wg_sem), (wu_hbm, wu, wu_sem))[kind]
        return pltpu.make_async_copy(src.at[0, :, pl.ds(c * FC, FC)], dst.at[c], sem.at[c])

    for c in range(NF):
        w_copy(0, c).start()
        w_copy(1, c).start()
    for c in range(n_tp * J):
        w_copy(2, c).start()

    def dev(ep, tp):
        return {"ep": ep, "tp": tp}

    barrier = pltpu.get_barrier_semaphore()
    for d in range(1, n_ep):
        pl.semaphore_signal(barrier, inc=1, device_id=dev(lax.rem(e + d, n_ep), t), device_id_type=MESH)
    for d in range(1, n_tp):
        pl.semaphore_signal(barrier, inc=1, device_id=dev(e, lax.rem(t + d, n_tp)), device_id_type=MESH)

    sub = lax.broadcasted_iota(jnp.int32, (rows, 128), 0)
    lane = lax.broadcasted_iota(jnp.int32, (rows, 128), 1)
    r = routes[...]
    wv = weights[...]
    for i in range(n_ep):
        col = jnp.sum(jnp.where(r == i, wv, 0.0), axis=1, keepdims=True)
        wsrc[i] = jnp.sum(jnp.where(sub == lane, col, 0.0), axis=0, keepdims=True)
    xg[e, t] = tok[...]
    wrow[e] = wsrc[e]

    pl.semaphore_wait(barrier, n_ep - 1 + n_tp - 1)

    def g_copy(kind, src, slot_e, target):
        return pltpu.make_async_remote_copy(
            src_ref=src, dst_ref=xg.at[slot_e, t], send_sem=gs.at[kind, slot_e],
            recv_sem=gr.at[slot_e, t], device_id=target, device_id_type=MESH)

    def targets(origin):
        res = []
        if origin in ("own", "low"):
            res.append((z < Z - 1, 0, dev(lax.rem(z + 1, Z) * X + x, t)))
        if origin in ("own", "high"):
            res.append((z > 0, 1, dev(lax.rem(z + Z - 1, Z) * X + x, t)))
        if origin != "across" and X > 1:
            res.append((None, 2, dev(z * X + xp, t)))
        for d in range(1, n_tp):
            res.append((None, 2 + d, dev(e, lax.rem(t + d, n_tp))))
        return res

    def forward(origin, slot_e, act):
        src = tok if origin == "own" else xg.at[slot_e, t]
        for cond, kind, target in targets(origin):
            cp = g_copy(kind, src, slot_e, target)
            fn = cp.start if act == "start" else cp.wait_send
            if cond is None:
                fn()
            else:
                pl.when(cond)(fn)

    def wait_slot(slot_e, slot_t):
        pltpu.make_async_remote_copy(
            src_ref=xg.at[slot_e, slot_t], dst_ref=xg.at[slot_e, slot_t], send_sem=gs.at[0, slot_e],
            recv_sem=gr.at[slot_e, slot_t], device_id=dev(e, t), device_id_type=MESH).wait_recv()

    def walk(act):
        forward("own", e, act)
        if act == "start":
            for d in range(1, n_ep):
                to = lax.rem(e + d, n_ep)
                pltpu.make_async_remote_copy(
                    src_ref=wsrc.at[to], dst_ref=wrow.at[e], send_sem=ws.at[to], recv_sem=wr.at[e],
                    device_id=dev(to, t), device_id_type=MESH).start()

        def handle(origin, slot_e):
            if act == "start":
                wait_slot(slot_e, t)
            forward(origin, slot_e, act)

        if X > 1:
            handle("across", z * X + xp)
        for d in range(1, Z):
            for origin, zz, cond in (("low", z - d, z >= d), ("high", z + d, z + d < Z)):
                pl.when(cond)(functools.partial(handle, origin, zz * X + x))
            if X > 1:
                for zz, cond in ((z - d, z >= d), (z + d, z + d < Z)):
                    pl.when(cond)(functools.partial(handle, "across", zz * X + xp))

    walk("start")

    def norm_step(i, carry):
        s = lax.rem(e + i, n_ep)

        @pl.when(i > 0)
        def _():
            pltpu.make_async_remote_copy(
                src_ref=wsrc.at[s], dst_ref=wrow.at[s], send_sem=ws.at[s], recv_sem=wr.at[s],
                device_id=dev(s, t), device_id_type=MESH).wait_recv()

        for d in range(1, n_tp):
            wait_slot(s, lax.rem(t + d, n_tp))
        parts = [xg[s, k].astype(F32) for k in range(n_tp)]
        width = w * n_tp
        mean = sum(jnp.sum(p, axis=1, keepdims=True) for p in parts) / width
        parts = [p - mean for p in parts]
        var = sum(jnp.sum(p * p, axis=1, keepdims=True) for p in parts) / width
        inv = lax.rsqrt(var + epsilon)
        at = pl.ds(pl.multiple_of(s * rows, rows), rows)
        for k in range(n_tp):
            normed[at, k * w:(k + 1) * w] = (parts[k] * inv * gain[:, k * w:(k + 1) * w]).astype(BF)
        wcol[at, :] = jnp.sum(jnp.where(sub == lane, wrow[s], 0.0), axis=1, keepdims=True)
        return carry

    lax.fori_loop(0, n_ep, norm_step, 0)

    def up_step(c, carry):
        w_copy(0, c).wait()
        gate_val = jnp.dot(normed[...], wg[c], preferred_element_type=F32)
        w_copy(1, c).wait()
        up_val = jnp.dot(normed[...], wu[c], preferred_element_type=F32)
        h = gate_val / (1.0 + jnp.exp(-gate_val)) * up_val * wcol[...]
        hidden[:, pl.ds(pl.multiple_of(c * FC, FC), FC)] = h.astype(BF)
        return carry

    lax.fori_loop(0, NF, up_step, 0)

    def p_copy(d, j):
        return pltpu.make_async_remote_copy(
            src_ref=psend.at[d - 1, j], dst_ref=precv.at[d - 1, j], send_sem=ps.at[d - 1, j],
            recv_sem=pr.at[d - 1, j], device_id=dev(e, lax.rem(t + d, n_tp)), device_id_type=MESH)

    def x_copy(j, zz):
        return pltpu.make_async_remote_copy(
            src_ref=xsend.at[j, zz], dst_ref=xrecv.at[j, zz], send_sem=xs.at[j, zz],
            recv_sem=xr.at[j, zz], device_id=dev(z * X + xp, t), device_id_type=MESH)

    def z_copy(j, d):
        return pltpu.make_async_remote_copy(
            src_ref=zsend.at[j, d - 1], dst_ref=zrecv.at[j, d - 1], send_sem=zs.at[j, d - 1],
            recv_sem=zr.at[j, d - 1], device_id=dev(lax.rem(z + d, Z) * X + x, t), device_id_type=MESH)

    def block(zz, xx):
        return pl.ds(pl.multiple_of((zz * X + xx) * rows, rows), rows)

    order = list(range(1, Z)) + [0]
    for d in list(range(1, n_tp)) + [0]:
        to = lax.rem(t + d, n_tp)
        for j in range(J):
            c = to * J + j
            w_copy(2, c).wait()
            acc = jnp.dot(hidden[...], wd[c], preferred_element_type=F32)
            if d:
                psend[d - 1, j] = acc.astype(BF)
                p_copy(d, j).start()
            else:
                for k in range(1, n_tp):
                    p_copy(k, j).wait_recv()
                    acc = acc + precv[k - 1, j].astype(F32)
                sacc[j] = acc
                if X > 1:
                    for dz in order:
                        zz = lax.rem(z + dz, Z)
                        xsend[j, zz] = sacc[j, block(zz, xp), :].astype(BF)
                        x_copy(j, zz).start()

    def summed(j, zz):
        total = sacc[j, block(zz, x), :]
        if X > 1:
            x_copy(j, zz).wait_recv()
            total = total + xrecv[j, zz].astype(F32)
        return total

    for j in range(J):
        for dz in range(1, Z):
            zsend[j, dz - 1] = summed(j, lax.rem(z + dz, Z)).astype(BF)
            z_copy(j, dz).start()
    for j in range(J):
        total = summed(j, z)
        for dz in range(1, Z):
            z_copy(j, dz).wait_recv()
            total = total + zrecv[j, dz - 1].astype(F32)
        out[:, j * CW:(j + 1) * CW] = total.astype(BF)

    walk("end")
    for d in range(1, n_ep):
        to = lax.rem(e + d, n_ep)
        pltpu.make_async_remote_copy(
            src_ref=wsrc.at[to], dst_ref=wrow.at[e], send_sem=ws.at[to], recv_sem=wr.at[e],
            device_id=dev(to, t), device_id_type=MESH).wait_send()
    for j in range(J):
        for d in range(1, n_tp):
            p_copy(d, j).wait_send()
        if X > 1:
            for zz in range(Z):
                x_copy(j, zz).wait_send()
        for dz in range(1, Z):
            z_copy(j, dz).wait_send()


def solution(mesh):
    n_ep, n_tp = mesh.shape["ep"], mesh.shape["tp"]
    X = 2 if n_ep % 2 == 0 else 1
    Z = n_ep // X

    def on_device(tokens, gain, routes, weights, w_gate, w_up, w_down):
        rows, w = tokens.shape
        D = w * n_tp
        top = routes.shape[1]
        F = w_gate.shape[2]
        FC = piece(F, 512)
        NF = F // FC
        CW = piece(w, 512)
        J = w // CW
        T = n_ep * rows
        dims = (n_ep, n_tp, X, Z, rows, w, FC, NF, CW, J, top)
        vm = pl.BlockSpec(memory_space=pltpu.VMEM)
        hbm = pl.BlockSpec(memory_space=pl.ANY)
        sem = pltpu.SemaphoreType.DMA
        tn, zn = max(n_tp - 1, 1), max(Z - 1, 1)
        return pl.pallas_call(
            functools.partial(kernel, dims),
            out_shape=jax.ShapeDtypeStruct((rows, w), BF),
            in_specs=[vm] * 4 + [hbm] * 3,
            out_specs=vm,
            scratch_shapes=[
                pltpu.VMEM((n_ep, n_tp, rows, w), BF),
                pltpu.VMEM((T, D), BF),
                pltpu.VMEM((T, F), BF),
                pltpu.VMEM((T, 1), F32),
                pltpu.VMEM((n_ep, 1, 128), F32),
                pltpu.VMEM((n_ep, 1, 128), F32),
                pltpu.VMEM((NF, D, FC), BF),
                pltpu.VMEM((NF, D, FC), BF),
                pltpu.VMEM((n_tp * J, F, CW), BF),
                pltpu.VMEM((tn, J, T, CW), BF),
                pltpu.VMEM((tn, J, T, CW), BF),
                pltpu.VMEM((J, T, CW), F32),
                pltpu.VMEM((J, Z, rows, CW), BF),
                pltpu.VMEM((J, Z, rows, CW), BF),
                pltpu.VMEM((J, zn, rows, CW), BF),
                pltpu.VMEM((J, zn, rows, CW), BF),
                sem((NF,)), sem((NF,)), sem((n_tp * J,)),
                sem((2 + n_tp, n_ep)), sem((n_ep, n_tp)),
                sem((n_ep,)), sem((n_ep,)),
                sem((tn, J)), sem((tn, J)),
                sem((J, Z)), sem((J, Z)),
                sem((J, zn)), sem((J, zn)),
            ],
            compiler_params=pltpu.CompilerParams(
                collective_id=0, has_side_effects=True, vmem_limit_bytes=62 << 20
            ),
        )(tokens, gain.reshape(1, -1), routes, weights, w_gate, w_up, w_down)

    in_specs = (
        P(("grp", "ep"), "tp"),
        P(),
        P(("grp", "ep"), None),
        P(("grp", "ep"), None),
        P("ep", None, "tp"),
        P("ep", None, "tp"),
        P("ep", "tp", None),
    )
    out_specs = P(("grp", "ep"), "tp")
    return jax.shard_map(
        on_device, mesh=mesh, in_specs=in_specs, out_specs=out_specs, check_vma=False
    )
```

time: 113 us -> 50.8 us (0.45)
  Pallas kernels: 0 us -> 46.3 us
  waiting for transfers between devices: 32.8 us -> 0 us
  matrix products: 27.1 us -> 0 us
  blocking collectives: 24.5 us -> 0 us
  between operations: 13.5 us -> 0.01 us
  starting transfers between devices: 5.82 us -> 0 us
  other arithmetic: 4.06 us -> 0 us
    pallas_call x0 -> x1, Pallas kernels: none -> 46.3 us  [on_device(): pl.pallas_call(functools.partial(kernel, dims), out_shape=jax.ShapeDtypeS...]
    dot_general x2 -> x0, matrix products: 27.1 us -> none  [the longest x1 17 us: expert_rows(): jnp.dot(hidden, down_w, preferred_element_type=jnp.float32)]
    all_to_all x1 -> x0, blocking collectives: 21.8 us -> none  [on_device(): lax.all_to_all(outbox, 'ep', split_axis=0, concat_axis=0, tiled=True)]
    all_to_all x1 -> x0, waiting for transfers between devices: 14.8 us -> none  [on_device(): lax.all_to_all(served, 'ep', split_axis=0, concat_axis=0, tiled=True)]
    reduce_scatter x1 -> x0, waiting for transfers between devices: 9.7 us -> none  [expert_rows(): lax.psum_scatter(partial_value, 'tp', scatter_dimension=1, tiled=True)]
    all_gather x1 -> x0, waiting for transfers between devices: 8.21 us -> none  [on_device(): lax.all_gather(lax.all_to_all(outbox, 'ep', split_axis=0, concat_axis=0,...]
    all_to_all x1 -> x0, starting transfers between devices: 5.78 us -> none  [on_device(): lax.all_to_all(served, 'ep', split_axis=0, concat_axis=0, tiled=True)]
    unnamed x6 -> x3, local copies, waits for them, and re-layouts: 0.86 us -> 4.2 us
  transfers between devices with their start and end apart: 3 -> 0, of which waited for: 3 -> 0; matrix products, arithmetic and copies ran while one was open for 0% -> 0% of each run, Pallas kernels for 0% -> 0%
where the time goes in v1:
time: 50.8 us; the launch traced here: 50.5 us
  Pallas kernels  46.3 us (91%)
  local copies, waits for them, and re-layouts  4.2 us (8%)
    pallas_call x1, Pallas kernels, on_device(): pl.pallas_call(functools.partial(kernel, dims), out_shape=jax.ShapeDtypeS...  46.3 us
    unnamed x3, local copies, waits for them, and re-layouts  4.2 us

profile of v1, /device:TPU:0, one launch (start us, length us, event | category | flops | bytes accessed | tf_op | source)
XLA Modules:
  0.0 50.5 jit_solution(7327856587100308032)
XLA Ops:
  0.0 1.4 %copy.8.routes = s32[32,4]{1,0:T(8,128)} copy(s32[32,4]{0,1:T(4,128)} %param.9) | data formatting | bytes 1024 | tf_op args[2]
  1.4 1.4 %copy.9.weights = f32[32,4]{1,0:T(8,128)} copy(f32[32,4]{0,1:T(4,128)} %param.10) | data formatting | bytes 1024 | tf_op args[3]
  2.7 46.3 %shard_map.73 = bf16[32,1024]{1,0:T(8,128)(2,1)} custom-call(bf16[32,1024]{1,0:T(8,128)(2,1)} %tok.1, f32[1,2048]{1,0:T(1,128)} %bitcast.1, s32[32,4]{1,0:T(8,128)} %copy.8.routes, f32[32,4]{1,0:T(8,128)} %copy.9.weights, bf16[1,2048,3072]{2,1,0:T(8,128)(2,1)} %wg_hbm.1, bf16[1,2048,3072]{2,1,0:T(8,128)(2,1)} %wu_hbm.1, bf16[1,3072,2048]{2,1,0:T(8,128)(2,1)} %wd_hbm.1), custom_call_target="tpu_custom_call" | custom-call | tf_op jit(solution)/shard_map/pallas_call | solution.py:254
  49.0 1.5 %copy.11 = bf16[32,1024]{1,0:T(8,128)(2,1)} copy(bf16[32,1024]{1,0:T(8,128)(2,1)} %shard_map.73) | data formatting | bytes 131072

commit v2 on v0

v2 whole, which is shorter than its diff:
```python
import functools

import jax
import jax.numpy as jnp
from jax import lax
from jax.experimental import pallas as pl
from jax.experimental.pallas import tpu as pltpu
from jax.sharding import PartitionSpec as P

epsilon = 1e-05
MESH = pl.DeviceIdType.MESH
BF = jnp.bfloat16
F32 = jnp.float32


def piece(total, most):
    best = 128
    for cand in range(128, min(total, most) + 1, 128):
        if total % cand == 0:
            best = cand
    return best


def kernel(dims, tok, gain, routes, weights, wg_hbm, wu_hbm, wd_hbm, out,
           xg, normed, hidden, wcol, wsrc, wrow, wg, wu, wd,
           psend, precv, sacc, xsend, xrecv, zsend, zrecv,
           wg_sem, wu_sem, wd_sem, gs, gr, ws, wr, ps, pr, xs, xr, zs, zr):
    n_ep, n_tp, X, Z, NB, rb, rows, w, FC, NF, CW, J = dims
    e = lax.axis_index("ep")
    t = lax.axis_index("tp")
    x = lax.rem(e, X)
    z = e // X
    xp = X - 1 - x

    def w_copy(kind, c):
        if kind == 2:
            return pltpu.make_async_copy(wd_hbm.at[0, :, pl.ds(c * CW, CW)], wd.at[c], wd_sem.at[c])
        src, dst, sem = ((wg_hbm, wg, wg_sem), (wu_hbm, wu, wu_sem))[kind]
        return pltpu.make_async_copy(src.at[0, :, pl.ds(c * FC, FC)], dst.at[c], sem.at[c])

    for c in range(NF):
        w_copy(0, c).start()
        w_copy(1, c).start()
    for c in range(n_tp * J):
        w_copy(2, c).start()

    def dev(ep, tp):
        return {"ep": ep, "tp": tp}

    barrier = pltpu.get_barrier_semaphore()
    for d in range(1, n_ep):
        pl.semaphore_signal(barrier, inc=1, device_id=dev(lax.rem(e + d, n_ep), t), device_id_type=MESH)
    for d in range(1, n_tp):
        pl.semaphore_signal(barrier, inc=1, device_id=dev(e, lax.rem(t + d, n_tp)), device_id_type=MESH)

    r = routes[...]
    wv = weights[...]
    for i in range(n_ep):
        wsrc[i] = jnp.sum(jnp.where(r == i, wv, 0.0), axis=0, keepdims=True)
    for b in range(NB):
        xg[b, e, t] = tok[b * rb:(b + 1) * rb]
    wrow[e] = wsrc[e]

    pl.semaphore_wait(barrier, n_ep - 1 + n_tp - 1)

    def g_copy(b, kind, src, slot_e, target):
        return pltpu.make_async_remote_copy(
            src_ref=src, dst_ref=xg.at[b, slot_e, t], send_sem=gs.at[b, kind, slot_e],
            recv_sem=gr.at[b, slot_e, t], device_id=target, device_id_type=MESH)

    def sends(b, origin, slot_e):
        src = tok.at[pl.ds(b * rb, rb)] if origin == "own" else xg.at[b, slot_e, t]
        res = []
        if origin == "own":
            for d in far:
                res.append(g_copy(b, d - 1, src, slot_e, dev(lax.rem(z + d, Z) * X + x, t)))
        if origin != "across" and X > 1:
            res.append(g_copy(b, Z - 1, src, slot_e, dev(z * X + xp, t)))
        for d in range(1, n_tp):
            res.append(g_copy(b, Z - 1 + d, src, slot_e, dev(e, lax.rem(t + d, n_tp))))
        return res

    def route_copy(to):
        return pltpu.make_async_remote_copy(
            src_ref=wsrc.at[to], dst_ref=wrow.at[e], send_sem=ws.at[to], recv_sem=wr.at[e],
            device_id=dev(to, t), device_id_type=MESH)

    def wait_slot(b, slot_e, slot_t):
        pltpu.make_async_remote_copy(
            src_ref=xg.at[b, slot_e, slot_t], dst_ref=xg.at[b, slot_e, slot_t], send_sem=gs.at[b, 0, slot_e],
            recv_sem=gr.at[b, slot_e, slot_t], device_id=dev(e, t), device_id_type=MESH).wait_recv()

    far = list(range(1, Z))

    def relay(b, origin, slot_e):
        wait_slot(b, slot_e, t)
        for cp in sends(b, origin, slot_e):
            cp.start()

    def relay_near(b):
        for d in far:
            relay(b, "along", lax.rem(z + d, Z) * X + x)

    def relay_across(b):
        if X > 1:
            for d in [0] + far:
                relay(b, "across", lax.rem(z + d, Z) * X + xp)

    def norm(b):
        diag = (lax.broadcasted_iota(jnp.int32, (rb, rows), 0) + b * rb
                == lax.broadcasted_iota(jnp.int32, (rb, rows), 1))

        def arrive(i, carry):
            s = lax.rem(e + i, n_ep)
            if b == 0:
                @pl.when(i > 0)
                def _():
                    pltpu.make_async_remote_copy(
                        src_ref=wsrc.at[s], dst_ref=wrow.at[s], send_sem=ws.at[s], recv_sem=wr.at[s],
                        device_id=dev(s, t), device_id_type=MESH).wait_recv()

            for d in range(1, n_tp):
                wait_slot(b, s, lax.rem(t + d, n_tp))
            return carry

        def norm_step(s, carry):
            parts = [xg[b, s, k].astype(F32) for k in range(n_tp)]
            width = w * n_tp
            mean = sum(jnp.sum(p, axis=1, keepdims=True) for p in parts) / width
            parts = [p - mean for p in parts]
            var = sum(jnp.sum(p * p, axis=1, keepdims=True) for p in parts) / width
            inv = lax.rsqrt(var + epsilon)
            at = pl.ds(pl.multiple_of(s * rb, rb), rb)
            for k in range(n_tp):
                normed[b, at, k * w:(k + 1) * w] = (
                    parts[k] * inv * gain[:, k * w:(k + 1) * w]).astype(BF)
            wcol[b, at, :] = jnp.sum(jnp.where(diag, wrow[s], 0.0), axis=1, keepdims=True)
            return carry

        lax.fori_loop(0, n_ep, arrive, 0)
        lax.fori_loop(0, n_ep, norm_step, 0, unroll=4)

    def up(b, between):
        def up_step(c, carry):
            if b == 0:
                w_copy(0, c).wait()
            gate_val = jnp.dot(normed[b], wg[c], preferred_element_type=F32)
            if b == 0:
                w_copy(1, c).wait()
            up_val = jnp.dot(normed[b], wu[c], preferred_element_type=F32)
            h = gate_val / (1.0 + jnp.exp(-gate_val)) * up_val * wcol[b]
            hidden[b, :, pl.ds(pl.multiple_of(c * FC, FC), FC)] = h.astype(BF)
            for at, fn in between:
                pl.when(c == min(at, NF - 1))(fn)
            return carry

        lax.fori_loop(0, NF, up_step, 0)

    def p_copy(b, d, j):
        return pltpu.make_async_remote_copy(
            src_ref=psend.at[b, d - 1, j], dst_ref=precv.at[b, d - 1, j], send_sem=ps.at[b, d - 1, j],
            recv_sem=pr.at[b, d - 1, j], device_id=dev(e, lax.rem(t + d, n_tp)), device_id_type=MESH)

    def x_copy(b, j, zz):
        return pltpu.make_async_remote_copy(
            src_ref=xsend.at[b, j, zz], dst_ref=xrecv.at[b, j, zz], send_sem=xs.at[b, j, zz],
            recv_sem=xr.at[b, j, zz], device_id=dev(z * X + xp, t), device_id_type=MESH)

    def z_copy(b, j, d):
        return pltpu.make_async_remote_copy(
            src_ref=zsend.at[b, j, d - 1], dst_ref=zrecv.at[b, j, d - 1], send_sem=zs.at[b, j, d - 1],
            recv_sem=zr.at[b, j, d - 1], device_id=dev(lax.rem(z + d, Z) * X + x, t), device_id_type=MESH)

    def block(zz, xx):
        return pl.ds(pl.multiple_of((zz * X + xx) * rb, rb), rb)

    def down(b):
        for j in range(J):
            for d in list(range(1, n_tp)) + [0]:
                to = lax.rem(t + d, n_tp)
                c = to * J + j
                if b == 0:
                    w_copy(2, c).wait()
                acc = jnp.dot(hidden[b], wd[c], preferred_element_type=F32)
                if d:
                    psend[b, d - 1, j] = acc.astype(BF)
                    p_copy(b, d, j).start()
                else:
                    for k in range(1, n_tp):
                        p_copy(b, k, j).wait_recv()
                        acc = acc + precv[b, k - 1, j].astype(F32)
                    sacc[b, j] = acc
                    if X > 1:
                        for dz in far + [0]:
                            zz = lax.rem(z + dz, Z)
                            xsend[b, j, zz] = sacc[b, j, block(zz, xp), :].astype(BF)
                            x_copy(b, j, zz).start()

    def summed(b, j, zz):
        total = sacc[b, j, block(zz, x), :]
        if X > 1:
            x_copy(b, j, zz).wait_recv()
            total = total + xrecv[b, j, zz].astype(F32)
        return total

    def along(b):
        for j in range(J):
            for dz in far:
                zsend[b, j, dz - 1] = summed(b, j, lax.rem(z + dz, Z)).astype(BF)
                z_copy(b, j, dz).start()

    def finish(b):
        for j in range(J):
            total = summed(b, j, z)
            for dz in far:
                z_copy(b, j, dz).wait_recv()
                total = total + zrecv[b, j, dz - 1].astype(F32)
            out[b * rb:(b + 1) * rb, j * CW:(j + 1) * CW] = total.astype(BF)

    def begin(b):
        for cp in sends(b, "own", e):
            cp.start()

    begin(0)
    for d in range(1, n_ep):
        route_copy(lax.rem(e + d, n_ep)).start()
    relay_near(0)
    for b in range(1, NB):
        begin(b)
    relay_across(0)
    norm(0)
    for b in range(NB):
        between = []
        if b > 0:
            between.append((NF - 1, functools.partial(along, b - 1)))
        if b + 1 < NB:
            between.append((NF // 2, functools.partial(relay_near, b + 1)))
            between.append((NF - 1, functools.partial(relay_across, b + 1)))
        up(b, between)
        if b + 1 < NB:
            norm(b + 1)
        down(b)
    along(NB - 1)
    for b in range(NB):
        finish(b)

    for b in range(NB):
        for cp in sends(b, "own", e):
            cp.wait_send()
        for d in far:
            for cp in sends(b, "along", lax.rem(z + d, Z) * X + x):
                cp.wait_send()
        if X > 1:
            for d in range(Z):
                for cp in sends(b, "across", lax.rem(z + d, Z) * X + xp):
                    cp.wait_send()
        for j in range(J):
            for d in range(1, n_tp):
                p_copy(b, d, j).wait_send()
            if X > 1:
                for zz in range(Z):
                    x_copy(b, j, zz).wait_send()
            for dz in far:
                z_copy(b, j, dz).wait_send()
    for d in range(1, n_ep):
        route_copy(lax.rem(e + d, n_ep)).wait_send()


def solution(mesh):
    n_ep, n_tp = mesh.shape["ep"], mesh.shape["tp"]
    X = 2 if n_ep % 2 == 0 else 1
    Z = n_ep // X

    def on_device(tokens, gain, routes, weights, w_gate, w_up, w_down):
        rows, w = tokens.shape
        D = w * n_tp
        F = w_gate.shape[2]
        FC = piece(F, 512)
        NF = F // FC
        CW = piece(w, 512)
        J = w // CW
        NB = 1
        rb = rows // NB
        T = n_ep * rb
        dims = (n_ep, n_tp, X, Z, NB, rb, rows, w, FC, NF, CW, J)
        vm = pl.BlockSpec(memory_space=pltpu.VMEM)
        hbm = pl.BlockSpec(memory_space=pl.ANY)
        sem = pltpu.SemaphoreType.DMA
        tn, zn = max(n_tp - 1, 1), max(Z - 1, 1)
        return pl.pallas_call(
            functools.partial(kernel, dims),
            out_shape=jax.ShapeDtypeStruct((rows, w), BF),
            in_specs=[vm] * 4 + [hbm] * 3,
            out_specs=vm,
            scratch_shapes=[
                pltpu.VMEM((NB, n_ep, n_tp, rb, w), BF),
                pltpu.VMEM((NB, T, D), BF),
                pltpu.VMEM((NB, T, F), BF),
                pltpu.VMEM((NB, T, 1), F32),
                pltpu.VMEM((n_ep, 1, rows), F32),
                pltpu.VMEM((n_ep, 1, rows), F32),
                pltpu.VMEM((NF, D, FC), BF),
                pltpu.VMEM((NF, D, FC), BF),
                pltpu.VMEM((n_tp * J, F, CW), BF),
                pltpu.VMEM((NB, tn, J, T, CW), BF),
                pltpu.VMEM((NB, tn, J, T, CW), BF),
                pltpu.VMEM((NB, J, T, CW), F32),
                pltpu.VMEM((NB, J, Z, rb, CW), BF),
                pltpu.VMEM((NB, J, Z, rb, CW), BF),
                pltpu.VMEM((NB, J, zn, rb, CW), BF),
                pltpu.VMEM((NB, J, zn, rb, CW), BF),
                sem((NF,)), sem((NF,)), sem((n_tp * J,)),
                sem((NB, Z + n_tp - 1, n_ep)), sem((NB, n_ep, n_tp)),
                sem((n_ep,)), sem((n_ep,)),
                sem((NB, tn, J)), sem((NB, tn, J)),
                sem((NB, J, Z)), sem((NB, J, Z)),
                sem((NB, J, zn)), sem((NB, J, zn)),
            ],
            compiler_params=pltpu.CompilerParams(
                collective_id=0, has_side_effects=True, vmem_limit_bytes=62 << 20
            ),
        )(tokens, gain.reshape(1, -1), routes.T, weights.T, w_gate, w_up, w_down)

    in_specs = (
        P(("grp", "ep"), "tp"),
        P(),
        P(("grp", "ep"), None),
        P(("grp", "ep"), None),
        P("ep", None, "tp"),
        P("ep", None, "tp"),
        P("ep", "tp", None),
    )
    out_specs = P(("grp", "ep"), "tp")
    return jax.shard_map(
        on_device, mesh=mesh, in_specs=in_specs, out_specs=out_specs, check_vma=False
    )
```

time: 113 us -> 46 us (0.41)
  Pallas kernels: 0 us -> 44.3 us
  waiting for transfers between devices: 32.8 us -> 0 us
  matrix products: 27.1 us -> 0 us
  blocking collectives: 24.5 us -> 0 us
  between operations: 13.5 us -> 0.01 us
  starting transfers between devices: 5.82 us -> 0 us
  other arithmetic: 4.06 us -> 0 us
  local copies, waits for them, and re-layouts: 5.08 us -> 1.47 us
    pallas_call x0 -> x1, Pallas kernels: none -> 44.3 us  [on_device(): pl.pallas_call(functools.partial(kernel, dims), out_shape=jax.ShapeDtypeS...]
    dot_general x2 -> x0, matrix products: 27.1 us -> none  [the longest x1 17 us: expert_rows(): jnp.dot(hidden, down_w, preferred_element_type=jnp.float32)]
    all_to_all x1 -> x0, blocking collectives: 21.8 us -> none  [on_device(): lax.all_to_all(outbox, 'ep', split_axis=0, concat_axis=0, tiled=True)]
    all_to_all x1 -> x0, waiting for transfers between devices: 14.8 us -> none  [on_device(): lax.all_to_all(served, 'ep', split_axis=0, concat_axis=0, tiled=True)]
    reduce_scatter x1 -> x0, waiting for transfers between devices: 9.7 us -> none  [expert_rows(): lax.psum_scatter(partial_value, 'tp', scatter_dimension=1, tiled=True)]
    all_gather x1 -> x0, waiting for transfers between devices: 8.21 us -> none  [on_device(): lax.all_gather(lax.all_to_all(outbox, 'ep', split_axis=0, concat_axis=0,...]
    all_to_all x1 -> x0, starting transfers between devices: 5.78 us -> none  [on_device(): lax.all_to_all(served, 'ep', split_axis=0, concat_axis=0, tiled=True)]
    psum x1 -> x0, blocking collectives: 2.63 us -> none  [on_device(): lax.psum((jnp.sum(values, axis=1), jnp.sum(values * values, axis=1)), 'tp')]
  transfers between devices with their start and end apart: 3 -> 0, of which waited for: 3 -> 0; matrix products, arithmetic and copies ran while one was open for 0% -> 0% of each run, Pallas kernels for 0% -> 0%
where the time goes in v2:
time: 46 us; the launch traced here: 45.8 us
  Pallas kernels  44.3 us (96%)
  local copies, waits for them, and re-layouts  1.47 us (3%)
    pallas_call x1, Pallas kernels, on_device(): pl.pallas_call(functools.partial(kernel, dims), out_shape=jax.ShapeDtypeS...  44.3 us
    unnamed x1, local copies, waits for them, and re-layouts  1.47 us

profile of v2, /device:TPU:0, one launch (start us, length us, event | category | flops | bytes accessed | tf_op | source)
XLA Modules:
  0.0 45.8 jit_solution(3324972482383600193)
XLA Ops:
  0.0 44.3 %shard_map.73 = bf16[32,1024]{1,0:T(8,128)(2,1)} custom-call(bf16[32,1024]{1,0:T(8,128)(2,1)} %tok.1, f32[1,2048]{1,0:T(1,128)} %bitcast.3, s32[4,32]{1,0:T(4,128)} %bitcast.4, f32[4,32]{1,0:T(4,128)} %bitcast.5, bf16[1,2048,3072]{2,1,0:T(8,128)(2,1)} %wg_hbm.1, bf16[1,2048,3072]{2,1,0:T(8,128)(2,1)} %wu_hbm.1, bf16[1,3072,2048]{2,1,0:T(8,128)(2,1)} %wd_hbm.1), custom_call_target="tpu_custom_call" | custom-call | tf_op jit(solution)/shard_map/pallas_call | solution.py:290
  44.3 1.5 %copy.9 = bf16[32,1024]{1,0:T(8,128)(2,1)} copy(bf16[32,1024]{1,0:T(8,128)(2,1)} %shard_map.73) | data formatting | bytes 131072
